TPU v7x, 32 devices: a whole 2x2x4 slice. The times are simulated.
32 devices in a mesh: sp: 8 (over z, x), tp: 4 (over y, core).
Axes of the slice: x: 2, y: 2, z: 4, core: 2. Of those that a mesh axis runs over, the one named last changes fastest.
Arguments:
- inputs: bfloat16 [4096, 2048], P('sp', 'tp'), may hold values from -45 to 45
- norm_gain: float32 [3, 2048], replicated, may hold values from 0.1 to 1.9
- w_value: bfloat16 [3, 2048, 1024], P(None, 'sp', 'tp'), may hold values from -0.125 to 0.125
- w_gate: bfloat16 [3, 2048, 1024], P(None, 'sp', 'tp'), may hold values from -0.125 to 0.125
- conv_taps: float32 [3, 31, 1024], P(None, None, 'tp'), may hold values from -5 to 5
- ln_gain: float32 [3, 1024], P(None, 'tp'), may hold values from 0.1 to 1.9
- ln_bias: float32 [3, 1024], P(None, 'tp'), may hold values from -3 to 3
- w_out: bfloat16 [3, 1024, 2048], P(None, 'tp', 'sp'), may hold values from -0.1875 to 0.1875
Outputs:
- stream: bfloat16 [4096, 2048], P('sp', 'tp')
All inputs are finite; a program needn't handle non-finite values.
Results may differ from a plain program's by a relative error of at most 0.01.
Values may be sent and summed in bfloat16 or wider, within the bound.
A program may use at most 64 MiB of HBM per device.

v0:
```python
import jax
import jax.numpy as jnp
from jax import lax
from jax.sharding import PartitionSpec as P


def from_behind(block, axis, distance):
    devices = range(lax.axis_size(axis))
    route = [(i - distance, i) for i in devices if i - distance in devices]
    return lax.ppermute(block, axis, route)


def shards(inputs, norm_gain, w_value, w_gate, conv_taps, ln_gain, ln_bias, w_out):
    rows = inputs.shape[0]
    reach = conv_taps.shape[1] - 1
    layers = conv_taps.shape[0]
    channels = conv_taps.shape[2] * lax.axis_size("tp")
    whole_value, whole_gate, whole_out = (
        lax.all_gather(w_value, "sp", axis=1, tiled=True),
        lax.all_gather(w_gate, "sp", axis=1, tiled=True),
        lax.all_gather(w_out, "sp", axis=2, tiled=True),
    )
    stream = inputs
    for layer in range(layers):
        full_rows = lax.all_gather(stream, "tp", axis=1, tiled=True)
        xf = full_rows.astype(jnp.float32)
        meansq = jnp.mean(xf * xf, axis=1, keepdims=True)
        hidden = (xf * lax.rsqrt(meansq + 1e-06) * norm_gain[layer][None, :]).astype(jnp.bfloat16)
        value = jnp.dot(hidden, whole_value[layer], preferred_element_type=jnp.float32)
        gate = jnp.dot(hidden, whole_gate[layer], preferred_element_type=jnp.float32)
        glu = (value * jax.nn.sigmoid(gate)).astype(jnp.bfloat16)
        rim = from_behind(glu[rows - reach :], "sp", 1)
        padded = jnp.concatenate([rim, glu], axis=0)
        count = padded.shape[0] - reach
        filtered = jnp.zeros((count, glu.shape[1]), jnp.float32)
        for tap in range(reach + 1):
            filtered = filtered + conv_taps[layer, tap][None, :] * padded[tap : tap + count].astype(
                jnp.float32
            )
        total_sum, total_sq = lax.psum(
            (jnp.sum(filtered, axis=1), jnp.sum(filtered * filtered, axis=1)), "tp"
        )
        mean_val = (total_sum / channels)[:, None]
        var_val = (total_sq / channels)[:, None] - mean_val * mean_val
        normed = jax.nn.silu(
            (filtered - mean_val) * lax.rsqrt(var_val + 1e-06) * ln_gain[layer][None, :]
            + ln_bias[layer][None, :]
        ).astype(jnp.bfloat16)
        partial_out = jnp.dot(normed, whole_out[layer], preferred_element_type=jnp.float32)
        summed = lax.psum_scatter(
            partial_out.astype(jnp.bfloat16), "tp", scatter_dimension=1, tiled=True
        ).astype(jnp.float32)
        kept = stream.astype(jnp.float32)
        stream = (kept + summed).astype(jnp.bfloat16)
    return stream


def solution(mesh):
    in_specs = (
        P("sp", "tp"),
        P(),
        P(None, "sp", "tp"),
        P(None, "sp", "tp"),
        P(None, None, "tp"),
        P(None, "tp"),
        P(None, "tp"),
        P(None, "tp", "sp"),
    )
    out_specs = P("sp", "tp")
    return jax.shard_map(shards, mesh=mesh, in_specs=in_specs, out_specs=out_specs, check_vma=False)
```

profile of v0, /device:TPU:0, one launch (start us, length us, event | category | flops | bytes accessed | tf_op | source)
XLA Modules:
  0.0 422.9 jit_solution(3484355526385756584)
XLA Ops:
  13.1 21.1 %all-gather.7.cloned.1.call-done = bf16[512,2048]{1,0:T(8,128)(2,1)} async-done(((bf16[512,512]{1,0:T(8,128)(2,1)}), bf16[512,2048]{1,0:T(8,128)(2,1)}) %all-gather.7.cloned.1.call-update) | async-done | bytes 2097168 | tf_op jit(solution)/shard_map/all_gather | solution.py:25
  34.2 2.1 fusion
  36.3 60.1 %all-gather.11.cloned.1.call-done = bf16[3,2048,256]{2,1,0:T(8,128)(2,1)} async-done(((bf16[3,256,256]{2,1,0:T(8,128)(2,1)}), bf16[3,2048,256]{2,1,0:T(8,128)(2,1)}) %all-gather.11.cloned.1.call-update) | async-done | bytes 3145744 | tf_op jit(solution)/shard_map/all_gather | solution.py:20
  96.4 2.8 fusion.17
  99.2 58.1 %all-gather.9.cloned.1.call-done = bf16[3,2048,256]{2,1,0:T(8,128)(2,1)} async-done(((bf16[3,256,256]{2,1,0:T(8,128)(2,1)}), bf16[3,2048,256]{2,1,0:T(8,128)(2,1)}) %all-gather.9.cloned.1.call-update) | async-done | bytes 3145744 | tf_op jit(solution)/shard_map/all_gather | solution.py:19
  157.4 2.0 fusion.18
  159.4 2.5 collective-permute-start
  163.3 2.4 fusion.134
  165.7 5.7 %all-reduce.2 = (f32[512]{0:T(512)S(1)}, f32[512]{0:T(512)S(1)}) all-reduce(f32[512]{0:T(512)S(1)} %get-tuple-element.10, f32[512]{0:T(512)S(1)} %get-tuple-element.9), channel_id=1, replica_groups=mesh['sp'=8,'tp'=4] {'tp'}, use_global_device_ids=true, to_apply=%region_4.0 | all-reduce | flops 1024 | bytes 8192 | tf_op jit(solution)/shard_map/psum | solution.py:40
  171.4 49.2 %all-gather.13.cloned.1.call-done = bf16[3,256,2048]{2,1,0:T(8,128)(2,1)} async-done(((bf16[3,256,256]{2,1,0:T(8,128)(2,1)}), bf16[3,256,2048]{2,1,0:T(8,128)(2,1)}) %all-gather.13.cloned.1.call-update) | async-done | bytes 3145744 | tf_op jit(solution)/shard_map/all_gather | solution.py:21
  220.6 3.4 convolution_convert_fusion.2
  224.1 29.5 %reduce-scatter.4.cloned.1.call-done = bf16[512,512]{1,0:T(8,128)(2,1)} async-done(((bf16[512,2048]{1,0:T(8,128)(2,1)}), bf16[512,512]{1,0:T(8,128)(2,1)}) %reduce-scatter.4.cloned.1.call-update) | async-done | bytes 524304 | tf_op jit(solution)/shard_map/reduce_scatter | solution.py:50
  253.6 2.0 add_convert_fusion.2
  255.6 22.6 %all-gather.15.cloned.1.call-done = bf16[512,2048]{1,0:T(8,128)(2,1)} async-done(((bf16[512,512]{1,0:T(8,128)(2,1)}), bf16[512,2048]{1,0:T(8,128)(2,1)}) %all-gather.15.cloned.1.call-update) | async-done | bytes 2097168 | tf_op jit(solution)/shard_map/all_gather | solution.py:25
  278.3 2.1 fusion.3
  280.4 2.8 fusion.14
  283.2 2.0 fusion.19
  285.2 3.4 collective-permute-start.1
  290.0 2.4 fusion.133
  292.4 6.0 %all-reduce.1 = (f32[512]{0:T(512)S(1)}, f32[512]{0:T(512)S(1)}) all-reduce(f32[512]{0:T(512)S(1)} %get-tuple-element.8, f32[512]{0:T(512)S(1)} %get-tuple-element.7), channel_id=1, replica_groups=mesh['sp'=8,'tp'=4] {'tp'}, use_global_device_ids=true, to_apply=%region_10.11 | all-reduce | flops 1024 | bytes 8192 | tf_op jit(solution)/shard_map/psum | solution.py:40
  298.4 3.4 convolution_convert_fusion.1
  301.9 32.1 %reduce-scatter.6.cloned.1.call-done = bf16[512,512]{1,0:T(8,128)(2,1)} async-done(((bf16[512,2048]{1,0:T(8,128)(2,1)}), bf16[512,512]{1,0:T(8,128)(2,1)}) %reduce-scatter.6.cloned.1.call-update) | async-done | bytes 524304 | tf_op jit(solution)/shard_map/reduce_scatter | solution.py:50
  334.0 2.0 add_convert_fusion.1
  336.0 22.7 %all-gather.17.cloned.1.call-done = bf16[512,2048]{1,0:T(8,128)(2,1)} async-done(((bf16[512,512]{1,0:T(8,128)(2,1)}), bf16[512,2048]{1,0:T(8,128)(2,1)}) %all-gather.17.cloned.1.call-update) | async-done | bytes 2097168 | tf_op jit(solution)/shard_map/all_gather | solution.py:25
  358.7 2.1 fusion.6
  360.8 2.8 fusion.11
  363.6 2.0 fusion.20
  365.6 3.6 collective-permute-start.2
  370.4 2.4 fusion.132
  372.8 5.9 %all-reduce = (f32[512]{0:T(512)S(1)}, f32[512]{0:T(512)S(1)}) all-reduce(f32[512]{0:T(512)S(1)} %get-tuple-element.6, f32[512]{0:T(512)S(1)} %get-tuple-element.5), channel_id=1, replica_groups=mesh['sp'=8,'tp'=4] {'tp'}, use_global_device_ids=true, to_apply=%region_16.17 | all-reduce | flops 1024 | bytes 8192 | tf_op jit(solution)/shard_map/psum | solution.py:40
  378.8 3.4 convolution_convert_fusion
  382.2 32.1 %reduce-scatter.8.cloned.1.call-done = bf16[512,512]{1,0:T(8,128)(2,1)} async-done(((bf16[512,2048]{1,0:T(8,128)(2,1)}), bf16[512,512]{1,0:T(8,128)(2,1)}) %reduce-scatter.8.cloned.1.call-update) | async-done | bytes 524304 | tf_op jit(solution)/shard_map/reduce_scatter | solution.py:50
  (55 shorter events, 12.9 us)
Async XLA Ops:
  6.5 27.7 %all-gather.7.cloned.1.call-start = ((), (), s32[]{:S(2)}) async-start(), calls=%async_computation.3 | async-start | bytes 2621440 | tf_op jit(solution)/shard_map/all_gather | solution.py:25
  7.3 89.2 %all-gather.11.cloned.1.call-start = ((), (), s32[]{:S(2)}) async-start(), calls=%async_computation.5 | async-start | bytes 3538944 | tf_op jit(solution)/shard_map/all_gather | solution.py:20
  8.0 149.3 %all-gather.9.cloned.1.call-start = ((), (), s32[]{:S(2)}) async-start(), calls=%async_computation.4 | async-start | bytes 3538944 | tf_op jit(solution)/shard_map/all_gather | solution.py:19
  8.7 211.9 %all-gather.13.cloned.1.call-start = ((), (), s32[]{:S(2)}) async-start(), calls=%async_computation.6 | async-start | bytes 3538944 | tf_op jit(solution)/shard_map/all_gather | solution.py:21
  9.3 244.2 %reduce-scatter.4.cloned.1.call-start = ((), (), s32[]{:S(2)}) async-start(), calls=%async_computation.7 | async-start | bytes 2621440 | tf_op jit(solution)/shard_map/reduce_scatter | solution.py:50
  96.4 60.9 %copy-start.3 = (bf16[512,2048]{1,0:T(8,128)(2,1)S(1)}, bf16[512,2048]{1,0:T(8,128)(2,1)}, u32[]{:S(2)}) copy-start(bf16[512,2048]{1,0:T(8,128)(2,1)} %all-gather.7.cloned.1.call-done) | copy-start | bytes 6291460
  99.2 62.6 %copy-start.7 = (f32[3,256]{1,0:T(4,128)S(1)}, f32[3,256]{1,0:T(4,128)}, u32[]{:S(2)}) copy-start(f32[3,256]{1,0:T(4,128)} %param.14) | copy-start | bytes 9220
  159.4 3.9 collective-permute-start
  220.6 33.0 %copy-start.2 = (bf16[512,512]{1,0:T(8,128)(2,1)S(1)}, bf16[512,512]{1,0:T(8,128)(2,1)}, u32[]{:S(2)}) copy-start(bf16[512,512]{1,0:T(8,128)(2,1)} %param.8) | copy-start | bytes 1572868
  224.0 31.6 %copy-start.6 = (f32[3,31,256]{2,1,0:T(8,128)S(1)}, f32[3,31,256]{2,1,0:T(8,128)}, u32[]{:S(2)}) copy-start(f32[3,31,256]{2,1,0:T(8,128)} %param.12) | copy-start | bytes 285700
  224.0 54.3 %all-gather.15.cloned.1.call-start = ((), (), s32[]{:S(2)}) async-start(), calls=%async_computation.8 | async-start | bytes 2621440 | tf_op jit(solution)/shard_map/all_gather | solution.py:25
  255.6 78.4 %reduce-scatter.6.cloned.1.call-start = ((), (), s32[]{:S(2)}) async-start(), calls=%async_computation.9 | async-start | bytes 2621440 | tf_op jit(solution)/shard_map/reduce_scatter | solution.py:50
  280.4 2.8 copy-start.4
  285.2 4.8 %collective-permute-start.1 = (bf16[30,256]{1,0:T(8,128)(2,1)S(1)}, bf16[30,256]{1,0:T(8,128)(2,1)S(1)}, u32[]{:S(2)}, u32[]{:S(2)}) collective-permute-start(bf16[30,256]{1,0:T(8,128)(2,1)S(1)} %slice.880), channel_id=1, source_target_pairs={{0,4},{4,8},{8,12},{12,16},{16,20},{20,24},{24,28},{1,5},{5,9},{9,... | collective-permute-start | bytes 46088 | tf_op jit(solution)/shard_map/ppermute | solution.py:10
  298.4 35.5 %copy-start = (bf16[512,512]{1,0:T(8,128)(2,1)S(1)}, bf16[512,512]{1,0:T(8,128)(2,1)}, u32[]{:S(2)}) copy-start(bf16[512,512]{1,0:T(8,128)(2,1)} %add_convert_fusion.2) | copy-start | bytes 1572868
  301.8 56.8 %all-gather.17.cloned.1.call-start = ((), (), s32[]{:S(2)}) async-start(), calls=%async_computation.10 | async-start | bytes 2621440 | tf_op jit(solution)/shard_map/all_gather | solution.py:25
  336.0 78.4 %reduce-scatter.8.cloned.1.call-start = ((), (), s32[]{:S(2)}) async-start(), calls=%async_computation.11 | async-start | bytes 2621440 | tf_op jit(solution)/shard_map/reduce_scatter | solution.py:50
  360.8 2.8 copy-start.5
  365.6 4.8 %collective-permute-start.2 = (bf16[30,256]{1,0:T(8,128)(2,1)S(1)}, bf16[30,256]{1,0:T(8,128)(2,1)S(1)}, u32[]{:S(2)}, u32[]{:S(2)}) collective-permute-start(bf16[30,256]{1,0:T(8,128)(2,1)S(1)} %slice.942), channel_id=1, source_target_pairs={{0,4},{4,8},{8,12},{12,16},{16,20},{20,24},{24,28},{1,5},{5,9},{9,... | collective-permute-start | bytes 46088 | tf_op jit(solution)/shard_map/ppermute | solution.py:10
  378.8 35.6 %copy-start.1 = (bf16[512,512]{1,0:T(8,128)(2,1)S(1)}, bf16[512,512]{1,0:T(8,128)(2,1)}, u32[]{:S(2)}) copy-start(bf16[512,512]{1,0:T(8,128)(2,1)} %add_convert_fusion.1) | copy-start | bytes 1572868
Sparse Core Ops, SparseCore 0:
  8.9 25.2 all-gather.6
  36.4 60.0 all-gather.10
  98.6 58.6 all-gather.8
  159.2 61.3 all-gather.12
  224.1 29.3 reduce-scatter.3
  255.7 22.5 all-gather.14
  302.0 31.9 reduce-scatter.5
  336.1 22.5 all-gather.16
  382.4 31.9 reduce-scatter.7
where the time goes:
time: 424 us; the launch traced here: 423 us
  waiting for transfers between devices  334 us (79%)
  matrix products  24.6 us (6%)
  other arithmetic  19.5 us (5%)
  blocking collectives  17.6 us (4%)
  between operations  13.4 us (3%)
  starting transfers between devices  9.7 us (2%)
    reduce_scatter x3, waiting for transfers between devices, shards(): lax.psum_scatter(partial_out.astype(jnp.bfloat16), 'tp', scatter_dimensio...  93.7 us
    all_gather x3, waiting for transfers between devices, shards(): full_rows = lax.all_gather(stream, 'tp', axis=1, tiled=True)  66.4 us
    all_gather x1, waiting for transfers between devices, shards(): lax.all_gather(w_gate, 'sp', axis=1, tiled=True)  60.1 us
    all_gather x1, waiting for transfers between devices, shards(): lax.all_gather(w_value, 'sp', axis=1, tiled=True)  58.1 us
    all_gather x1, waiting for transfers between devices, shards(): lax.all_gather(w_out, 'sp', axis=2, tiled=True)  49.2 us
    psum x3, blocking collectives, shards(): lax.psum((jnp.sum(filtered, axis=1), jnp.sum(filtered * filtered, axis=1)...  17.6 us
    dot_general x3, matrix products, shards(): jnp.dot(normed, whole_out[layer], preferred_element_type=jnp.float32)  10.2 us
    ppermute x3, starting transfers between devices, from_behind(): return lax.ppermute(block, axis, route)  9.38 us
  transfers between devices with their start and end apart: 12, of which 12 were waited for; matrix products, arithmetic and copies ran while one was open for 3% of the time, Pallas kernels for 0%

commit v1 on v0

--- a/solution.py
+++ b/solution.py
@@ -1,7 +1,427 @@
+import functools
+
 import jax
 import jax.numpy as jnp
 from jax import lax
+from jax.experimental import pallas as pl
+from jax.experimental.pallas import tpu as pltpu
 from jax.sharding import PartitionSpec as P
+
+MESH = pl.DeviceIdType.MESH
+PAIR = 2
+CHUNK = 128
+HALO = 32
+LANES = 128
+
+
+def fused_kernel(
+    n_sp, n_tp, eps,
+    x_ref, gain_ref, wv_ref, wg_ref, taps_ref, lng_ref, lnb_ref, wo_ref,
+    out_ref,
+    wv_all, wg_all, wo_all, xf, hid, glu, filt, rim_out, rim_in, stat,
+    ps_out, ps_in, keep, fs_out, fs_in,
+    w_recv, w_zsend, w_xsend, ag_recv, ag_send, rim_s, rim_r, st_recv, st_send,
+    ps_s, ps_r, fs_s, fs_r,
+):
+    sp = lax.axis_index("sp")
+    tp = lax.axis_index("tp")
+    layers, depth = wv_ref.shape[0], wv_ref.shape[1]
+    rows, dblk = x_ref.shape
+    width = wo_ref.shape[2]
+    chan = wv_ref.shape[2]
+    taps = taps_ref.shape[1]
+    features = dblk * n_tp
+    channels = chan * n_tp
+    n_chunks = rows // CHUNK
+    n_out = n_sp // PAIR
+    per_blk = dblk // width
+    outer, inner = lax.div(sp, PAIR), lax.rem(sp, PAIR)
+    x_peer = outer * PAIR + (PAIR - 1 - inner)
+    far_half, core = lax.div(tp, PAIR), lax.rem(tp, PAIR)
+    partner = far_half * PAIR + (PAIR - 1 - core)
+    far = (n_tp // PAIR - 1 - far_half) * PAIR + core
+    far_partner = (n_tp // PAIR - 1 - far_half) * PAIR + (PAIR - 1 - core)
+    first_off = HALO - (taps - 1)
+    halves = chan // LANES
+
+    barrier = pltpu.get_barrier_semaphore()
+    for step in range(1, n_sp):
+        pl.semaphore_signal(barrier, inc=1, device_id=(lax.rem(sp + step, n_sp), tp), device_id_type=MESH)
+    for step in range(1, n_tp):
+        pl.semaphore_signal(barrier, inc=1, device_id=(sp, lax.rem(tp + step, n_tp)), device_id_type=MESH)
+    pl.semaphore_wait(barrier, n_sp - 1 + n_tp - 1)
+
+    def chunk_rows(c):
+        return pl.ds(pl.multiple_of(c * CHUNK, CHUNK), CHUNK)
+
+    def remote(src, dst, send, recv, sp_to, tp_to):
+        return pltpu.make_async_remote_copy(
+            src_ref=src, dst_ref=dst, send_sem=send, recv_sem=recv,
+            device_id=(sp_to, tp_to), device_id_type=MESH,
+        )
+
+    w_in = (wv_ref, wg_ref, wo_ref)
+
+    def w_slot(m, l, s):
+        if m == 2:
+            return wo_all.at[l, s]
+        return (wv_all, wg_all)[m].at[l, pl.ds(pl.multiple_of(s * depth, depth), depth), :]
+
+    def z_copy(m, l, j):
+        to = lax.rem(outer + j, n_out) * PAIR + inner
+        return remote(w_in[m].at[l], w_slot(m, l, sp), w_zsend.at[l, m, j], w_recv.at[l, m, sp], to, tp)
+
+    def z_arrival(m, l, j):
+        s = lax.rem(outer + j, n_out) * PAIR + inner
+        return remote(w_in[m].at[l], w_slot(m, l, s), w_zsend.at[l, m, j], w_recv.at[l, m, s], s, tp)
+
+    def x_copy(m, l, j):
+        s = lax.rem(outer + j, n_out) * PAIR + inner
+        src = w_in[m].at[l] if j == 0 else w_slot(m, l, s)
+        return remote(src, w_slot(m, l, s), w_xsend.at[l, m, j], w_recv.at[l, m, s], x_peer, tp)
+
+    def x_arrival(m, l, j):
+        s = lax.rem(outer + j, n_out) * PAIR + (PAIR - 1 - inner)
+        return remote(w_in[m].at[l], w_slot(m, l, s), w_xsend.at[l, m, j], w_recv.at[l, m, s], x_peer, tp)
+
+    def z_send_all(m, l):
+        for j in range(1, n_out):
+            z_copy(m, l, j).start()
+
+    def relay(m, l):
+        for j in range(1, n_out):
+            z_arrival(m, l, j).wait_recv()
+            x_copy(m, l, j).start()
+
+    def w_ready(m, l):
+        for j in range(n_out):
+            x_arrival(m, l, j).wait_recv()
+
+    def ag_far(c):
+        r = chunk_rows(c)
+        return remote(xf.at[tp, r, :], xf.at[tp, r, :], ag_send.at[0, c], ag_recv.at[0, c], sp, far)
+
+    def ag_partner(c):
+        r = chunk_rows(c)
+        return remote(xf.at[tp, r, :], xf.at[tp, r, :], ag_send.at[1, c], ag_recv.at[1, c], sp, partner)
+
+    def ag_forward(c):
+        r = chunk_rows(c)
+        return remote(xf.at[far, r, :], xf.at[far, r, :], ag_send.at[2, c], ag_recv.at[2, c], sp, partner)
+
+    def stat_copy(l, c, step):
+        to = lax.rem(tp + step, n_tp)
+        return remote(stat.at[l, c, tp], stat.at[l, c, tp], st_send.at[c, step], st_recv.at[c, tp], sp, to)
+
+    def stat_arrival(l, c, step):
+        src = lax.rem(tp + step, n_tp)
+        return remote(stat.at[l, c, src], stat.at[l, c, src], st_send.at[c, step], st_recv.at[c, src], sp, src)
+
+    def ps_copy(c):
+        r = chunk_rows(c)
+        return remote(ps_out.at[:, r, :], ps_in.at[:, r, :], ps_s.at[c], ps_r.at[c], sp, partner)
+
+    def fs_copy(c):
+        r = chunk_rows(c)
+        return remote(fs_out.at[r, :], fs_in.at[r, :], fs_s.at[c], fs_r.at[c], sp, far)
+
+    def rim_copy(l):
+        to = lax.rem(sp + 1, n_sp)
+        return remote(rim_out.at[l], rim_in.at[l], rim_s.at[l], rim_r.at[l], to, tp)
+
+    xf[tp] = x_ref[...]
+    for c in range(n_chunks):
+        ag_far(c).start()
+        ag_partner(c).start()
+    for m in range(3):
+        z_send_all(m, 0)
+        x_copy(m, 0, 0).start()
+
+    def own_weights(l, carry):
+        own = pl.ds(pl.multiple_of(sp * depth, depth), depth)
+        wv_all[l, own, :] = wv_ref[l]
+        wg_all[l, own, :] = wg_ref[l]
+        wo_all[l, sp] = wo_ref[l]
+        return carry
+
+    lax.fori_loop(0, layers, own_weights, 0)
+
+    relay(0, 0)
+    relay(1, 0)
+
+    def do_glu(l, c):
+        ag_partner(c).wait_recv()
+        ag_forward(c).wait_recv()
+        r = chunk_rows(c)
+        blocks = [xf[b, r, :].astype(jnp.float32) for b in range(n_tp)]
+        total = sum(jnp.sum(b * b, axis=1, keepdims=True) for b in blocks)
+        scale = lax.rsqrt(total / features + eps)
+        for b in range(n_tp):
+            cols = slice(b * dblk, (b + 1) * dblk)
+            hid[:, cols] = (xf[b, r, :].astype(jnp.float32) * scale * gain_ref[l, :, cols]).astype(jnp.bfloat16)
+        h = hid[...]
+        value = jnp.dot(h, wv_all[l], preferred_element_type=jnp.float32)
+        gate = jnp.dot(h, wg_all[l], preferred_element_type=jnp.float32)
+        g = (value * jax.nn.sigmoid(gate)).astype(jnp.bfloat16)
+        for k in range(halves):
+            glu[k, pl.ds(pl.multiple_of(HALO + c * CHUNK, HALO), CHUNK), :] = g[:, k * LANES:(k + 1) * LANES].astype(jnp.float32)
+
+        @pl.when((c == n_chunks - 1) & (sp < n_sp - 1))
+        def _():
+            rim_out[l] = g[CHUNK - HALO:, :]
+            rim_copy(l).start()
+
+    def do_conv(l, c):
+        @pl.when((c == 0) & (sp > 0))
+        def _():
+            rim_copy(l).wait_recv()
+            rim = rim_in[l].astype(jnp.float32)
+            for k in range(halves):
+                glu[k, 0:HALO, :] = rim[:, k * LANES:(k + 1) * LANES]
+
+        @pl.when((c == 0) & (sp == 0))
+        def _():
+            glu[:, 0:HALO, :] = jnp.zeros((halves, HALO, LANES), jnp.float32)
+
+        r = chunk_rows(c)
+        sums = jnp.zeros((CHUNK, 1), jnp.float32)
+        squares = jnp.zeros((CHUNK, 1), jnp.float32)
+        for k in range(halves):
+            acc = jnp.zeros((CHUNK, LANES), jnp.float32)
+            for tap in range(taps):
+                acc = acc + taps_ref[l, tap:tap + 1, k * LANES:(k + 1) * LANES] * glu[
+                    k, pl.ds(c * CHUNK + first_off + tap, CHUNK), :]
+            filt[r, k * LANES:(k + 1) * LANES] = acc
+            sums = sums + jnp.sum(acc, axis=1, keepdims=True)
+            squares = squares + jnp.sum(acc * acc, axis=1, keepdims=True)
+        lane = lax.broadcasted_iota(jnp.int32, (CHUNK, LANES), 1)
+        both = jnp.where(lane == 0, sums, squares)
+        stat[l, c, tp] = jnp.transpose(both)[0:8, :]
+        for step in range(1, n_tp):
+            stat_copy(l, c, step).start()
+
+    def do_out(l, c):
+        for step in range(1, n_tp):
+            stat_arrival(l, c, step).wait_recv()
+        r = chunk_rows(c)
+        tot = stat[l, c, 0]
+        for b in range(1, n_tp):
+            tot = tot + stat[l, c, b]
+        tot = jnp.transpose(jnp.concatenate([tot, jnp.zeros((LANES - 8, CHUNK), jnp.float32)], axis=0))
+        mean = tot[:, 0:1] / channels
+        var = tot[:, 1:2] / channels - mean * mean
+        pre = (filt[r, :] - mean) * lax.rsqrt(var + eps) * lng_ref[l] + lnb_ref[l]
+        normed = jax.nn.silu(pre).astype(jnp.bfloat16)
+        for step in range(1, n_tp):
+            stat_copy(l, c, step).wait_send()
+        ag_far(c).wait_send()
+        ag_partner(c).wait_send()
+        ag_forward(c).wait_send()
+        for half in range(n_tp // PAIR):
+            for q in range(per_blk):
+                cols = slice(q * width, (q + 1) * width)
+                away = (half * PAIR + (PAIR - 1 - core)) * per_blk + q
+                ps_out[half, r, cols] = jnp.dot(
+                    normed, wo_all[l, away], preferred_element_type=jnp.float32).astype(jnp.bfloat16)
+        ps_copy(c).start()
+        for half in range(n_tp // PAIR):
+            for q in range(per_blk):
+                cols = slice(q * width, (q + 1) * width)
+                mine = (half * PAIR + core) * per_blk + q
+                keep[half, r, cols] = jnp.dot(normed, wo_all[l, mine], preferred_element_type=jnp.float32)
+
+    def do_pair(l, c):
+        ps_copy(c).wait_recv()
+        r = chunk_rows(c)
+        other = n_tp // PAIR - 1 - far_half
+        fs_out[r, :] = (keep[other, r, :] + ps_in[other, r, :].astype(jnp.float32)).astype(jnp.bfloat16)
+        fs_copy(c).start()
+
+    def do_final(l, c):
+        fs_copy(c).wait_recv()
+        ps_copy(c).wait_send()
+        fs_copy(c).wait_send()
+        r = chunk_rows(c)
+        branch = keep[far_half, r, :] + ps_in[far_half, r, :].astype(jnp.float32) + fs_in[r, :].astype(jnp.float32)
+        new = (xf[tp, r, :].astype(jnp.float32) + branch).astype(jnp.bfloat16)
+
+        @pl.when(l < layers - 1)
+        def _():
+            xf[tp, r, :] = new
+            ag_far(c).start()
+            ag_partner(c).start()
+
+        @pl.when(l == layers - 1)
+        def _():
+            out_ref[r, :] = new
+
+    def layer_body(l, carry):
+        base = lax.rem(l, n_chunks)
+        more = l < layers - 1
+
+        @pl.when(more)
+        def _():
+            for m in range(3):
+                z_send_all(m, l + 1)
+
+        w_ready(0, l)
+        w_ready(1, l)
+
+        def step_body(i, inner_carry):
+            def at(back):
+                return lax.rem(base + i + n_chunks * 2 - back, n_chunks)
+
+            @pl.when(i < n_chunks)
+            def _():
+                ag_far(at(0)).wait_recv()
+                ag_forward(at(0)).start()
+
+            @pl.when((i >= 2) & (i < n_chunks + 2))
+            def _():
+                do_conv(l, at(1))
+
+            @pl.when(i < n_chunks)
+            def _():
+                do_glu(l, at(0))
+
+            @pl.when(i == 2)
+            def _():
+                relay(2, l)
+
+            @pl.when(i == 3)
+            def _():
+                w_ready(2, l)
+
+            @pl.when((i >= 3) & (i < n_chunks + 3))
+            def _():
+                do_out(l, at(2))
+
+            @pl.when((i >= 4) & (i < n_chunks + 4))
+            def _():
+                do_pair(l, at(3))
+
+            @pl.when(more & (i == n_chunks))
+            def _():
+                for m in range(3):
+                    x_copy(m, l + 1, 0).start()
+
+            @pl.when(more & (i == n_chunks + 2))
+            def _():
+                relay(0, l + 1)
+
+            @pl.when(i >= 5)
+            def _():
+                do_final(l, at(4))
+
+            return inner_carry
+
+        lax.fori_loop(0, n_chunks + 5, step_body, 0)
+
+        @pl.when(more)
+        def _():
+            relay(1, l + 1)
+
+        return carry
+
+    lax.fori_loop(0, layers, layer_body, 0)
+
+    def drain(l, carry):
+        for m in range(3):
+            for j in range(1, n_out):
+                z_copy(m, l, j).wait_send()
+            for j in range(n_out):
+                x_copy(m, l, j).wait_send()
+
+        @pl.when(sp < n_sp - 1)
+        def _():
+            rim_copy(l).wait_send()
+
+        return carry
+
+    lax.fori_loop(0, layers, drain, 0)
+
+
+def fused_shards(n_sp, n_tp, inputs, norm_gain, w_value, w_gate, conv_taps, ln_gain, ln_bias, w_out):
+    layers, depth, chan = w_value.shape
+    rows, dblk = inputs.shape
+    width = w_out.shape[2]
+    n_chunks = rows // CHUNK
+    features = dblk * n_tp
+    n_half = n_tp // PAIR
+    bf16, f32 = jnp.bfloat16, jnp.float32
+    dma = pltpu.SemaphoreType.DMA
+    vmem = pl.BlockSpec(memory_space=pltpu.VMEM)
+    return pl.pallas_call(
+        functools.partial(fused_kernel, n_sp, n_tp, 1e-06),
+        out_shape=jax.ShapeDtypeStruct((rows, dblk), bf16),
+        in_specs=[vmem] * 8,
+        out_specs=vmem,
+        scratch_shapes=[
+            pltpu.VMEM((layers, n_sp * depth, chan), bf16),
+            pltpu.VMEM((layers, n_sp * depth, chan), bf16),
+            pltpu.VMEM((layers, n_sp, chan, width), bf16),
+            pltpu.VMEM((n_tp, rows, dblk), bf16),
+            pltpu.VMEM((CHUNK, features), bf16),
+            pltpu.VMEM((chan // LANES, HALO + rows, LANES), f32),
+            pltpu.VMEM((rows, chan), f32),
+            pltpu.VMEM((layers, HALO, chan), bf16),
+            pltpu.VMEM((layers, HALO, chan), bf16),
+            pltpu.VMEM((layers, n_chunks, n_tp, 8, CHUNK), f32),
+            pltpu.VMEM((n_half, rows, dblk), bf16),
+            pltpu.VMEM((n_half, rows, dblk), bf16),
+            pltpu.VMEM((n_half, rows, dblk), f32),
+            pltpu.VMEM((rows, dblk), bf16),
+            pltpu.VMEM((rows, dblk), bf16),
+            dma((layers, 3, n_sp)),
+            dma((layers, 3, n_sp // PAIR)),
+            dma((layers, 3, n_sp // PAIR)),
+            dma((3, n_chunks)),
+            dma((3, n_chunks)),
+            dma((layers,)),
+            dma((layers,)),
+            dma((n_chunks, n_tp)),
+            dma((n_chunks, n_tp)),
+            dma((n_chunks,)),
+            dma((n_chunks,)),
+            dma((n_chunks,)),
+            dma((n_chunks,)),
+        ],
+        compiler_params=pltpu.CompilerParams(collective_id=0, has_side_effects=True),
+    )(
+        inputs,
+        norm_gain.reshape(layers, 1, features),
+        w_value,
+        w_gate,
+        conv_taps,
+        ln_gain.reshape(layers, 1, chan),
+        ln_bias.reshape(layers, 1, chan),
+        w_out,
+    )
+
+
+def fits_kernel(n_sp, n_tp, inputs, w_value, conv_taps, w_out):
+    rows, dblk = inputs.shape
+    width = w_out.shape[2]
+    return (
+        n_sp % PAIR == 0
+        and n_sp > PAIR
+        and n_tp == PAIR * PAIR
+        and rows % CHUNK == 0
+        and rows // CHUNK >= 2
+        and w_value.shape[1] % LANES == 0
+        and w_value.shape[2] % LANES == 0
+        and width % LANES == 0
+        and dblk % width == 0
+        and conv_taps.shape[1] - 1 <= HALO
+    )
+
+
+def shards(inputs, norm_gain, w_value, w_gate, conv_taps, ln_gain, ln_bias, w_out):
+    n_sp, n_tp = lax.axis_size("sp"), lax.axis_size("tp")
+    args = (inputs, norm_gain, w_value, w_gate, conv_taps, ln_gain, ln_bias, w_out)
+    if fits_kernel(n_sp, n_tp, inputs, w_value, conv_taps, w_out):
+        return fused_shards(n_sp, n_tp, *args)
+    return plain_shards(*args)
 
 
 def from_behind(block, axis, distance):
@@ -10,7 +430,7 @@
     return lax.ppermute(block, axis, route)
 
 
-def shards(inputs, norm_gain, w_value, w_gate, conv_taps, ln_gain, ln_bias, w_out):
+def plain_shards(inputs, norm_gain, w_value, w_gate, conv_taps, ln_gain, ln_bias, w_out):
     rows = inputs.shape[0]
     reach = conv_taps.shape[1] - 1
     layers = conv_taps.shape[0]

time: 424 us -> 187 us (0.44)
  the two profiles are of different devices: /device:TPU:0 before, /device:TPU:16 now
where the time goes in v1:
time: 187 us
  Pallas kernels  182 us (97%)
  local copies, waits for them, and re-layouts  5.14 us (3%)
    pallas_call x1, Pallas kernels, fused_shards(): pl.pallas_call(functools.partial(fused_kernel, n_sp, n_tp, 1e-06), out_sh...  182 us

profile of v1, /device:TPU:16, one launch (start us, length us, event | category | flops | bytes accessed | tf_op | source)
XLA Modules:
  0.0 187.0 jit_solution(2279228816823322990)
XLA Ops:
  0.0 0.0 copy-start
  0.0 1.3 reshape.10.lng_ref
  1.3 0.0 copy-done
  1.3 0.6 reshape.11.lnb_ref
  1.9 1.4 reshape.9.gain_ref
  3.3 181.9 %shard_map.82 = bf16[512,512]{1,0:T(8,128)(2,1)} custom-call(bf16[512,512]{1,0:T(8,128)(2,1)} %x_ref.1, f32[3,1,2048]{2,1,0:T(1,128)} %reshape.9.gain_ref, bf16[3,256,256]{2,1,0:T(8,128)(2,1)} %wv_ref.1, bf16[3,256,256]{2,1,0:T(8,128)(2,1)} %wg_ref.1, f32[3,31,256]{2,1,0:T(8,128)} %taps_ref.1, f32[3,1,256]{2,1,0:T(1,128)} %reshape.10.lng_ref, ...), custom_call_target="tpu_custom_call" | custom-call | tf_op jit(solution)/shard_map/pallas_call | solution.py:354
  185.2 1.9 copy.10
Async XLA Ops:
  0.0 1.3 copy-start

commit v2 on v1

--- a/solution.py
+++ b/solution.py
@@ -12,6 +12,7 @@
 CHUNK = 128
 HALO = 32
 LANES = 128
+SIDE = (1,)
 
 
 def fused_kernel(
@@ -67,35 +68,75 @@
             return wo_all.at[l, s]
         return (wv_all, wg_all)[m].at[l, pl.ds(pl.multiple_of(s * depth, depth), depth), :]
 
+    last = n_out - 1
+    upper = lax.div(outer, n_out // 2)
+    near_end = outer + upper * (last - 2 * outer)
+
+    def line(j):
+        near = j + 1 - (near_end if j == 0 else 0)
+        return near + upper * (last - 2 * near)
+
     def z_copy(m, l, j):
-        to = lax.rem(outer + j, n_out) * PAIR + inner
+        to = line(j) * PAIR + inner
         return remote(w_in[m].at[l], w_slot(m, l, sp), w_zsend.at[l, m, j], w_recv.at[l, m, sp], to, tp)
 
     def z_arrival(m, l, j):
-        s = lax.rem(outer + j, n_out) * PAIR + inner
+        s = line(j) * PAIR + inner
         return remote(w_in[m].at[l], w_slot(m, l, s), w_zsend.at[l, m, j], w_recv.at[l, m, s], s, tp)
 
+    def z_forward(m, l):
+        s = line(last - 1) * PAIR + inner
+        to = upper * last * PAIR + inner
+        slot = w_slot(m, l, s)
+        return remote(slot, slot, w_zsend.at[l, m, last], w_recv.at[l, m, s], to, tp)
+
+    def x_own(m, l):
+        return remote(w_in[m].at[l], w_slot(m, l, sp), w_xsend.at[l, m, last], w_recv.at[l, m, sp], x_peer, tp)
+
     def x_copy(m, l, j):
-        s = lax.rem(outer + j, n_out) * PAIR + inner
-        src = w_in[m].at[l] if j == 0 else w_slot(m, l, s)
-        return remote(src, w_slot(m, l, s), w_xsend.at[l, m, j], w_recv.at[l, m, s], x_peer, tp)
-
-    def x_arrival(m, l, j):
-        s = lax.rem(outer + j, n_out) * PAIR + (PAIR - 1 - inner)
-        return remote(w_in[m].at[l], w_slot(m, l, s), w_xsend.at[l, m, j], w_recv.at[l, m, s], x_peer, tp)
+        s = line(j) * PAIR + inner
+        slot = w_slot(m, l, s)
+        return remote(slot, slot, w_xsend.at[l, m, j], w_recv.at[l, m, s], x_peer, tp)
+
+    def x_arrival(m, l, z):
+        s = z * PAIR + (PAIR - 1 - inner)
+        slot = w_slot(m, l, s)
+        return remote(slot, slot, w_xsend.at[l, m, last], w_recv.at[l, m, s], x_peer, tp)
+
+    def side_copy(m, l):
+        to = line(0) * PAIR + inner
+        slot = w_slot(m, l, x_peer)
+        return remote(slot, slot, w_xsend.at[l, m, 0], w_recv.at[l, m, x_peer], to, tp)
 
     def z_send_all(m, l):
-        for j in range(1, n_out):
+        for j in range(last - 1):
             z_copy(m, l, j).start()
 
+        @pl.when(near_end == 1)
+        def _():
+            z_copy(m, l, last - 1).start()
+
+    def relay_piece(m, l, j):
+        z_arrival(m, l, j).wait_recv()
+        if j == 0 and m in SIDE:
+            x_arrival(m, l, outer).wait_recv()
+            side_copy(m, l).start()
+        else:
+            x_copy(m, l, j).start()
+        if j == last - 1:
+            @pl.when(near_end == 1)
+            def _():
+                z_forward(m, l).start()
+
     def relay(m, l):
-        for j in range(1, n_out):
-            z_arrival(m, l, j).wait_recv()
-            x_copy(m, l, j).start()
+        for j in range(last):
+            relay_piece(m, l, j)
 
     def w_ready(m, l):
-        for j in range(n_out):
-            x_arrival(m, l, j).wait_recv()
+        if m not in SIDE:
+            x_arrival(m, l, outer).wait_recv()
+        for j in range(last):
+            x_arrival(m, l, line(j)).wait_recv()
 
     def ag_far(c):
         r = chunk_rows(c)
@@ -133,9 +174,10 @@
     for c in range(n_chunks):
         ag_far(c).start()
         ag_partner(c).start()
+    for m in range(2):
+        z_send_all(m, 0)
     for m in range(3):
-        z_send_all(m, 0)
-        x_copy(m, 0, 0).start()
+        x_own(m, 0).start()
 
     def own_weights(l, carry):
         own = pl.ds(pl.multiple_of(sp * depth, depth), depth)
@@ -146,8 +188,12 @@
 
     lax.fori_loop(0, layers, own_weights, 0)
 
+    z_send_all(2, 0)
     relay(0, 0)
+    x_own(0, 1).start()
+    z_send_all(0, 1)
     relay(1, 0)
+    x_own(1, 1).start()
 
     def do_glu(l, c):
         ag_partner(c).wait_recv()
@@ -158,7 +204,7 @@
         scale = lax.rsqrt(total / features + eps)
         for b in range(n_tp):
             cols = slice(b * dblk, (b + 1) * dblk)
-            hid[:, cols] = (xf[b, r, :].astype(jnp.float32) * scale * gain_ref[l, :, cols]).astype(jnp.bfloat16)
+            hid[:, cols] = (xf[b, r, :].astype(jnp.float32) * scale * gain_ref[pl.ds(l, 1), cols]).astype(jnp.bfloat16)
         h = hid[...]
         value = jnp.dot(h, wv_all[l], preferred_element_type=jnp.float32)
         gate = jnp.dot(h, wg_all[l], preferred_element_type=jnp.float32)
@@ -210,7 +256,7 @@
         tot = jnp.transpose(jnp.concatenate([tot, jnp.zeros((LANES - 8, CHUNK), jnp.float32)], axis=0))
         mean = tot[:, 0:1] / channels
         var = tot[:, 1:2] / channels - mean * mean
-        pre = (filt[r, :] - mean) * lax.rsqrt(var + eps) * lng_ref[l] + lnb_ref[l]
+        pre = (filt[r, :] - mean) * lax.rsqrt(var + eps) * lng_ref[pl.ds(l, 1), :] + lnb_ref[pl.ds(l, 1), :]
         normed = jax.nn.silu(pre).astype(jnp.bfloat16)
         for step in range(1, n_tp):
             stat_copy(l, c, step).wait_send()
@@ -259,11 +305,6 @@
         base = lax.rem(l, n_chunks)
         more = l < layers - 1
 
-        @pl.when(more)
-        def _():
-            for m in range(3):
-                z_send_all(m, l + 1)
-
         w_ready(0, l)
         w_ready(1, l)
 
@@ -271,6 +312,22 @@
             def at(back):
                 return lax.rem(base + i + n_chunks * 2 - back, n_chunks)
 
+            for k, (m, ahead) in enumerate(((2, 0), (0, 1), (1, 1))):
+                z_next, z_ahead = (m + 2) % 3, ahead + (m + 2) // 3
+
+                @pl.when((i == k * last) & (l + z_ahead < layers))
+                def _():
+                    z_send_all(z_next, l + z_ahead)
+
+                @pl.when((i == k * last) & (l + ahead + 1 < layers))
+                def _():
+                    x_own(m, l + ahead + 1).start()
+
+                for j in range(last):
+                    @pl.when((i == k * last + j) & (l + ahead < layers))
+                    def _():
+                        relay_piece(m, l + ahead, j)
+
             @pl.when(i < n_chunks)
             def _():
                 ag_far(at(0)).wait_recv()
@@ -284,10 +341,6 @@
             def _():
                 do_glu(l, at(0))
 
-            @pl.when(i == 2)
-            def _():
-                relay(2, l)
-
             @pl.when(i == 3)
             def _():
                 w_ready(2, l)
@@ -300,15 +353,6 @@
             def _():
                 do_pair(l, at(3))
 
-            @pl.when(more & (i == n_chunks))
-            def _():
-                for m in range(3):
-                    x_copy(m, l + 1, 0).start()
-
-            @pl.when(more & (i == n_chunks + 2))
-            def _():
-                relay(0, l + 1)
-
             @pl.when(i >= 5)
             def _():
                 do_final(l, at(4))
@@ -316,10 +360,6 @@
             return inner_carry
 
         lax.fori_loop(0, n_chunks + 5, step_body, 0)
-
-        @pl.when(more)
-        def _():
-            relay(1, l + 1)
 
         return carry
 
@@ -327,10 +367,17 @@
 
     def drain(l, carry):
         for m in range(3):
-            for j in range(1, n_out):
+            for j in range(last - 1):
                 z_copy(m, l, j).wait_send()
-            for j in range(n_out):
-                x_copy(m, l, j).wait_send()
+
+            @pl.when(near_end == 1)
+            def _():
+                z_copy(m, l, last - 1).wait_send()
+                z_forward(m, l).wait_send()
+
+            for j in range(last):
+                (side_copy(m, l) if j == 0 and m in SIDE else x_copy(m, l, j)).wait_send()
+            x_own(m, l).wait_send()
 
         @pl.when(sp < n_sp - 1)
         def _():
@@ -389,12 +436,12 @@
         compiler_params=pltpu.CompilerParams(collective_id=0, has_side_effects=True),
     )(
         inputs,
-        norm_gain.reshape(layers, 1, features),
+        norm_gain,
         w_value,
         w_gate,
         conv_taps,
-        ln_gain.reshape(layers, 1, chan),
-        ln_bias.reshape(layers, 1, chan),
+        ln_gain,
+        ln_bias,
         w_out,
     )
 
@@ -403,11 +450,11 @@
     rows, dblk = inputs.shape
     width = w_out.shape[2]
     return (
-        n_sp % PAIR == 0
-        and n_sp > PAIR
+        n_sp == 4 * PAIR
         and n_tp == PAIR * PAIR
         and rows % CHUNK == 0
-        and rows // CHUNK >= 2
+        and rows // CHUNK >= 4
+        and w_value.shape[0] >= 2
         and w_value.shape[1] % LANES == 0
         and w_value.shape[2] % LANES == 0
         and width % LANES == 0

time: 187 us -> 143 us (0.76)
  the two profiles are of different devices: /device:TPU:16 before, /device:TPU:0 now
where the time goes in v2:
time: 143 us; the launch traced here: 142 us
  Pallas kernels  140 us (98%)
  local copies, waits for them, and re-layouts  1.87 us (1%)
    pallas_call x1, Pallas kernels, fused_shards(): pl.pallas_call(functools.partial(fused_kernel, n_sp, n_tp, 1e-06), out_sh...  140 us

profile of v2, /device:TPU:0, one launch (start us, length us, event | category | flops | bytes accessed | tf_op | source)
XLA Modules:
  0.0 142.4 jit_solution(12631567291777740705)
XLA Ops:
  0.0 140.5 %shard_map.82 = bf16[512,512]{1,0:T(8,128)(2,1)} custom-call(bf16[512,512]{1,0:T(8,128)(2,1)} %x_ref.1, f32[3,2048]{1,0:T(4,128)} %gain_ref.1, bf16[3,256,256]{2,1,0:T(8,128)(2,1)} %wv_ref.1, bf16[3,256,256]{2,1,0:T(8,128)(2,1)} %wg_ref.1, f32[3,31,256]{2,1,0:T(8,128)} %taps_ref.1, f32[3,256]{1,0:T(4,128)} %lng_ref.1, f32[3,256]{1,0:T(4,128)} %lnb_ref.1, ...), custom_call_target="tpu_custom_call" | custom-call | tf_op jit(solution)/shard_map/pallas_call | solution.py:401
  140.5 1.9 %copy.10 = bf16[512,512]{1,0:T(8,128)(2,1)} copy(bf16[512,512]{1,0:T(8,128)(2,1)} %shard_map.82) | data formatting | bytes 1048576

commit v3 on v2

--- a/solution.py
+++ b/solution.py
@@ -12,6 +12,9 @@
 CHUNK = 128
 HALO = 32
 LANES = 128
+FIRST = 6
+Z_AHEAD, X_AHEAD = 1, 2
+STEPS = (0, 1, 2, 4, 5, 6, 7, 8, 8)
 SIDE = (1,)
 
 
@@ -50,6 +53,16 @@
         pl.semaphore_signal(barrier, inc=1, device_id=(lax.rem(sp + step, n_sp), tp), device_id_type=MESH)
     for step in range(1, n_tp):
         pl.semaphore_signal(barrier, inc=1, device_id=(sp, lax.rem(tp + step, n_tp)), device_id_type=MESH)
+    xf[tp] = x_ref[...]
+
+    def own_weights(l, carry):
+        own = pl.ds(pl.multiple_of(sp * depth, depth), depth)
+        wv_all[l, own, :] = wv_ref[l]
+        wg_all[l, own, :] = wg_ref[l]
+        wo_all[l, sp] = wo_ref[l]
+        return carry
+
+    lax.fori_loop(0, layers, own_weights, 0)
     pl.semaphore_wait(barrier, n_sp - 1 + n_tp - 1)
 
     def chunk_rows(c):
@@ -170,30 +183,19 @@
         to = lax.rem(sp + 1, n_sp)
         return remote(rim_out.at[l], rim_in.at[l], rim_s.at[l], rim_r.at[l], to, tp)
 
-    xf[tp] = x_ref[...]
     for c in range(n_chunks):
         ag_far(c).start()
         ag_partner(c).start()
-    for m in range(2):
-        z_send_all(m, 0)
-    for m in range(3):
-        x_own(m, 0).start()
-
-    def own_weights(l, carry):
-        own = pl.ds(pl.multiple_of(sp * depth, depth), depth)
-        wv_all[l, own, :] = wv_ref[l]
-        wg_all[l, own, :] = wg_ref[l]
-        wo_all[l, sp] = wo_ref[l]
-        return carry
-
-    lax.fori_loop(0, layers, own_weights, 0)
-
-    z_send_all(2, 0)
-    relay(0, 0)
-    x_own(0, 1).start()
-    z_send_all(0, 1)
-    relay(1, 0)
-    x_own(1, 1).start()
+    for q in range(Z_AHEAD):
+        z_send_all(q % 3, q // 3)
+    for q in range(X_AHEAD):
+        x_own(q % 3, q // 3).start()
+    for p in range(FIRST):
+        q, j = divmod(p, last)
+        if j == 0:
+            z_send_all((q + Z_AHEAD) % 3, (q + Z_AHEAD) // 3)
+            x_own((q + X_AHEAD) % 3, (q + X_AHEAD) // 3).start()
+        relay_piece(q % 3, q // 3, j)
 
     def do_glu(l, c):
         ag_partner(c).wait_recv()
@@ -305,33 +307,36 @@
         base = lax.rem(l, n_chunks)
         more = l < layers - 1
 
-        w_ready(0, l)
-        w_ready(1, l)
-
         def step_body(i, inner_carry):
             def at(back):
                 return lax.rem(base + i + n_chunks * 2 - back, n_chunks)
 
-            for k, (m, ahead) in enumerate(((2, 0), (0, 1), (1, 1))):
-                z_next, z_ahead = (m + 2) % 3, ahead + (m + 2) // 3
-
-                @pl.when((i == k * last) & (l + z_ahead < layers))
+            for k in range(3 * last):
+                q, j = divmod(FIRST + k, last)
+                if j == 0:
+                    z_next, x_next = q + Z_AHEAD, q + X_AHEAD
+
+                    @pl.when((i == STEPS[k]) & (l + z_next // 3 < layers))
+                    def _():
+                        z_send_all(z_next % 3, l + z_next // 3)
+
+                    @pl.when((i == STEPS[k]) & (l + x_next // 3 < layers))
+                    def _():
+                        x_own(x_next % 3, l + x_next // 3).start()
+
+                @pl.when((i == STEPS[k]) & (l + q // 3 < layers))
                 def _():
-                    z_send_all(z_next, l + z_ahead)
-
-                @pl.when((i == k * last) & (l + ahead + 1 < layers))
-                def _():
-                    x_own(m, l + ahead + 1).start()
-
-                for j in range(last):
-                    @pl.when((i == k * last + j) & (l + ahead < layers))
-                    def _():
-                        relay_piece(m, l + ahead, j)
+                    relay_piece(q % 3, l + q // 3, j)
 
             @pl.when(i < n_chunks)
             def _():
                 ag_far(at(0)).wait_recv()
                 ag_forward(at(0)).start()
+
+            @pl.when(i == 0)
+            def _():
+                w_ready(0, l)
+                w_ready(1, l)
 
             @pl.when((i >= 2) & (i < n_chunks + 2))
             def _():

time: 143 us -> 137 us (0.958)
  Pallas kernels: 140 us -> 135 us
    pallas_call x1, Pallas kernels: 140 us -> 135 us  [fused_shards(): pl.pallas_call(functools.partial(fused_kernel, n_sp, n_tp, 1e-06), out_sh...]
where the time goes in v3:
time: 137 us; the launch traced here: 136 us
  Pallas kernels  135 us (99%)
  local copies, waits for them, and re-layouts  1.87 us (1%)
    pallas_call x1, Pallas kernels, fused_shards(): pl.pallas_call(functools.partial(fused_kernel, n_sp, n_tp, 1e-06), out_sh...  135 us

profile of v3, /device:TPU:0, one launch (start us, length us, event | category | flops | bytes accessed | tf_op | source)
XLA Modules:
  0.0 136.4 jit_solution(2052734988583237710)
XLA Ops:
  0.0 134.5 %shard_map.82 = bf16[512,512]{1,0:T(8,128)(2,1)} custom-call(bf16[512,512]{1,0:T(8,128)(2,1)} %x_ref.1, f32[3,2048]{1,0:T(4,128)} %gain_ref.1, bf16[3,256,256]{2,1,0:T(8,128)(2,1)} %wv_ref.1, bf16[3,256,256]{2,1,0:T(8,128)(2,1)} %wg_ref.1, f32[3,31,256]{2,1,0:T(8,128)} %taps_ref.1, f32[3,256]{1,0:T(4,128)} %lng_ref.1, f32[3,256]{1,0:T(4,128)} %lnb_ref.1, ...), custom_call_target="tpu_custom_call" | custom-call | tf_op jit(solution)/shard_map/pallas_call | solution.py:406
  134.5 1.9 %copy.10 = bf16[512,512]{1,0:T(8,128)(2,1)} copy(bf16[512,512]{1,0:T(8,128)(2,1)} %shard_map.82) | data formatting | bytes 1048576
